TPU v7x, 512 devices: a whole 4x8x8 slice. The times are simulated.
512 devices in a mesh: sp: 32 (over z, x), tp: 16 (over y, core).
Axes of the slice: x: 4, y: 8, z: 8, core: 2. Of those that a mesh axis runs over, the one named last changes fastest.
Arguments:
- outer_gate: bfloat16 [512, 12288], P('tp', 'sp'), may hold values from -6 to 6
- inner_gate: bfloat16 [512, 12288], P('tp', 'sp'), may hold values from -6 to 6
- conv_input: bfloat16 [512, 12288], P('tp', 'sp'), may hold values from -6 to 6
- conv_taps: bfloat16 [3, 512], P(None, 'tp'), may hold values from -3.5 to 3.5
- mix_weight: bfloat16 [512, 2048], P(None, 'tp'), may hold values from -0.25 to 0.25
- residual: bfloat16 [12288, 2048], P('sp', 'tp'), may hold values from -24 to 24
- norm_gain: bfloat16 [2048], P('tp'), may hold values from 0.099609375 to 1.8984375
- routes: int32 [12288, 2], P('sp'), may hold values from 0 to 63, all different within a row; in each aligned block of 384 rows (0 to 383, 384 to 767, ...) at most 24 rows name the same one
- route_scores: float32 [12288, 2], P('sp'), may hold values from 0.05 to 1
- expert_gate: bfloat16 [64, 2048, 2048], P('sp', None, 'tp'), may hold values from -0.125 to 0.125
- expert_up: bfloat16 [64, 2048, 2048], P('sp', None, 'tp'), may hold values from -0.125 to 0.125
- expert_down: bfloat16 [64, 2048, 2048], P('sp', None, 'tp'), may hold values from -0.125 to 0.125
- shared_gate: bfloat16 [2048, 512], P(None, 'tp'), may hold values from -0.125 to 0.125
- shared_up: bfloat16 [2048, 512], P(None, 'tp'), may hold values from -0.125 to 0.125
- shared_down: bfloat16 [512, 2048], P(None, 'tp'), may hold values from -0.25 to 0.25
Outputs:
- layer_out: bfloat16 [12288, 2048], P('sp', 'tp')
Inputs may be any that keep to these rules, and one draw needn't show every extreme that they name: `routes`: within the rows of one index of sp (384 tokens), no expert is named by more than 24 of the token and choice pairs, a bound that some block reaches; the experts of one token differ.
All inputs are finite; a program needn't handle non-finite values.
Results may differ from a plain program's by a relative error of at most 0.014.
Values may be sent and summed in bfloat16 or wider, within the bound.
No kernel may reach another device: no remote copies, remote signals or barrier semaphores. Data moves between devices by JAX's collectives and lax.ppermute only.
A program may use at most 64 MiB of HBM per device.

v0:
```python
import jax
import jax.numpy as jnp
from jax import lax
from jax.sharding import PartitionSpec as P

D = 2048
epsilon = 1e-06
routed_scale = 2.5


def extended(array, sides, width):
    for axis, dim in sides:
        peers, length = (lax.axis_size(axis), array.shape[dim])
        up = [(i, (i + 1) % peers) for i in range(peers - 1)]
        down = [(j, i) for i, j in up]
        last = lax.slice_in_dim(array, length - width, length, axis=dim)
        first = lax.slice_in_dim(array, 0, width, axis=dim)
        before = lax.ppermute(last, axis, up)
        after = lax.ppermute(first, axis, down)
        array = jnp.concatenate([before, array, after], axis=dim)
    return array


def copy_for_each(array, axis):
    peers = lax.axis_size(axis)
    return lax.all_to_all(
        jnp.broadcast_to(array[None], (peers, *array.shape)), axis, 0, 0, tiled=True
    )


def taken_together(array, axis):
    return copy_for_each(array, axis).sum(axis=0)


def slot_tables(routes_block, expert_count, capacity):
    count_rows, top_count = routes_block.shape
    flat_route = routes_block.reshape(-1)
    onehot = (flat_route[:, None] == jnp.arange(expert_count, dtype=jnp.int32)[None, :]).astype(
        jnp.int32
    )
    before = jnp.cumsum(onehot, axis=0) - onehot
    position = jnp.sum(before * onehot, axis=1)
    slot_index = flat_route * capacity + position
    token_ids = jnp.arange(count_rows * top_count, dtype=jnp.int32) // top_count
    owners = jnp.full((expert_count * capacity,), -1, jnp.int32).at[slot_index].set(token_ids)
    return (slot_index.reshape(count_rows, top_count), owners)


def local(
    outer_gate,
    inner_gate,
    conv_input,
    conv_taps,
    mix_weight,
    residual,
    norm_gain,
    routes,
    route_scores,
    expert_gate,
    expert_up,
    expert_down,
    shared_gate,
    shared_up,
    shared_down,
):
    product = (inner_gate.astype(jnp.float32) * conv_input.astype(jnp.float32)).astype(jnp.bfloat16)
    padded = extended(product, (("sp", 1),), 1).astype(jnp.float32)
    kernel = conv_taps.astype(jnp.float32)
    filtered = (
        kernel[0][:, None] * padded[:, :-2]
        + kernel[1][:, None] * padded[:, 1:-1]
        + kernel[2][:, None] * padded[:, 2:]
    )
    mixed = (outer_gate.astype(jnp.float32) * filtered).astype(jnp.bfloat16)
    token_count = mixed.shape[1]
    rows_w = mix_weight
    projected = lax.dot_general(
        lax.all_gather(mixed, "tp", axis=0, tiled=True),
        rows_w,
        (((0,), (0,)), ((), ())),
        preferred_element_type=jnp.float32,
    )
    stream = (residual.astype(jnp.float32) + projected).astype(jnp.bfloat16)
    levels = stream.astype(jnp.float32)
    squares = taken_together(jnp.sum(levels * levels, axis=1), "tp")
    inverse_rms = lax.rsqrt(squares / D + epsilon)
    normed = (levels * inverse_rms[:, None] * norm_gain.astype(jnp.float32)).astype(jnp.bfloat16)
    whole_rows = lax.all_gather(normed, "tp", axis=1, tiled=True)
    shared_act = (
        jax.nn.silu(jnp.dot(whole_rows, shared_gate, preferred_element_type=jnp.float32))
        * jnp.dot(whole_rows, shared_up, preferred_element_type=jnp.float32)
    ).astype(jnp.bfloat16)
    rows_w = shared_down
    shared_out = jnp.dot(
        lax.all_gather(shared_act, "tp", axis=1, tiled=True),
        rows_w,
        preferred_element_type=jnp.float32,
    )
    group_count = lax.axis_size("sp")
    local_experts = expert_gate.shape[0]
    expert_count = local_experts * group_count
    capacity = 2 * token_count * routes.shape[1] // expert_count
    slot_index, owners = slot_tables(routes, expert_count, capacity)
    filled = owners >= 0
    source_ids = jnp.maximum(owners, 0)
    outgoing = jnp.where(filled[:, None], normed[source_ids], jnp.zeros((), jnp.bfloat16)).reshape(
        group_count, local_experts * capacity, -1
    )
    sliced = lax.all_to_all(outgoing, "sp", split_axis=0, concat_axis=1, tiled=True)
    received = lax.all_gather(sliced, "tp", axis=2, tiled=True)
    arrived = (
        received.reshape(group_count, local_experts, capacity, -1)
        .transpose(1, 0, 2, 3)
        .reshape(local_experts, group_count * capacity, -1)
    )
    gate_act = jnp.einsum("erd,edf->erf", arrived, expert_gate, preferred_element_type=jnp.float32)
    up_act = jnp.einsum("erd,edf->erf", arrived, expert_up, preferred_element_type=jnp.float32)
    hidden = (jax.nn.silu(gate_act) * up_act).astype(jnp.bfloat16)
    rows_w = expert_down
    expert_rows = jnp.einsum(
        "erf,efd->erd",
        lax.all_gather(hidden, "tp", axis=2, tiled=True),
        rows_w,
        preferred_element_type=jnp.float32,
    ).astype(jnp.bfloat16)
    feature_count = expert_rows.shape[2]
    regrouped = (
        expert_rows.reshape(local_experts, group_count, capacity, feature_count)
        .transpose(1, 0, 2, 3)
        .reshape(1, group_count * local_experts * capacity, feature_count)
    )
    returned = lax.all_to_all(regrouped, "sp", split_axis=1, concat_axis=0, tiled=True)
    flat_rows = returned.reshape(expert_count * capacity, feature_count)
    picked = flat_rows[slot_index].astype(jnp.float32)
    weights = route_scores / jnp.sum(route_scores, axis=1, keepdims=True) * routed_scale
    routed = jnp.einsum("tk,tkd->td", weights, picked)
    return (levels + routed + shared_out).astype(jnp.bfloat16)


def solution(mesh):
    in_specs = (
        P("tp", "sp"),
        P("tp", "sp"),
        P("tp", "sp"),
        P(None, "tp"),
        P(None, "tp"),
        P("sp", "tp"),
        P("tp"),
        P("sp", None),
        P("sp", None),
        P("sp", None, "tp"),
        P("sp", None, "tp"),
        P("sp", None, "tp"),
        P(None, "tp"),
        P(None, "tp"),
        P(None, "tp"),
    )
    out_specs = P("sp", "tp")
    return jax.shard_map(local, mesh=mesh, in_specs=in_specs, out_specs=out_specs, check_vma=False)
```

profile of v0, /device:TPU:1, one launch (start us, length us, event | category | flops | bytes accessed | tf_op | source)
XLA Modules:
  0.0 281.1 jit_solution(13468960967642711488)
XLA Ops:
  6.5 0.9 multiply_convert_fusion.1
  7.5 3.9 %collective-permute-start = (bf16[32,1]{1,0:T(8,128)(2,1)S(1)}, bf16[32,1]{1,0:T(8,128)(2,1)S(1)}, u32[]{:S(2)}, u32[]{:S(2)}) collective-permute-start(bf16[32,1]{1,0:T(8,128)(2,1)S(1)} %get-tuple-element.7), channel_id=1, source_target_pairs={{0,16},{16,32},{32,48},{48,64},{64,80},{80,96},{96,112},{112,128},... | collective-permute-start | bytes 200 | tf_op jit(solution)/shard_map/ppermute | solution.py:18
  11.4 1.3 collective-permute-start.1
  12.7 0.8 copy.64
  13.5 0.1 eq.29
  13.7 0.1 eq.25
  13.9 1.8 reduce-window.6
  15.7 0.3 slice_reduce_fusion
  16.0 0.1 fusion.7
  16.1 0.2 reduce_sum.45
  16.3 0.2 mul.110
  16.5 3.4 %scatter_custom_fusion = s32[1536]{0:T(1024)S(1)} fusion(s32[768]{0:T(1024)S(1)} %fusion.18, s32[768]{0:T(1024)S(1)} %add_select_fusion, s32[]{:T(128)} %constant.23.clone.1), kind=kCustom, calls=%fused_computation.49 | custom fusion | bytes 6148 | tf_op jit(solution)/shard_map/scatter | solution.py:45
  19.9 0.7 convert_element_type.58
  20.6 1.0 copy.63
  21.7 0.8 fusion.11
  22.6 19.5 %all_gather.15 = bf16[512,384]{1,0:T(8,128)(2,1)S(1)} all-gather(bf16[32,384]{1,0:T(8,128)(2,1)S(1)} %fusion.11), channel_id=1, replica_groups=mesh['sp'=32,'tp'=16] {'tp'}, dimensions={0}, use_global_device_ids=true | all-gather | bytes 417792 | tf_op jit(solution)/shard_map/all_gather | solution.py:78
  42.0 1.2 multiply_reduce_fusion.1
  43.2 0.6 broadcast_in_dim.38
  43.9 4.5 %all-to-all-start = ((f32[16,1,384]{2,1,0:T(1,128)}), f32[16,1,384]{2,1,0:T(1,128)S(1)}, u32[]{:S(2)}, u32[]{:S(2)}) async-start(f32[16,1,384]{2,1,0:T(1,128)} %broadcast_in_dim.38), calls=%async_computation | async-start | bytes 49152 | tf_op jit(solution)/shard_map/all_to_all | solution.py:26
  48.4 0.7 convert_element_type.68
  49.2 6.6 %all-to-all-done = f32[16,1,384]{2,1,0:T(1,128)S(1)} async-done(((f32[16,1,384]{2,1,0:T(1,128)}), f32[16,1,384]{2,1,0:T(1,128)S(1)}, u32[]{:S(2)}, u32[]{:S(2)}) %all-to-all-start) | async-done | bytes 24608 | tf_op jit(solution)/shard_map/all_to_all | solution.py:26
  56.0 3.2 %gather_fusion = bf16[1536,128]{1,0:T(8,128)(2,1)S(1)} fusion(bf16[384,128]{1,0:T(8,128)(2,1)S(1)} %copy.69, s32[2048]{0:T(1024)S(1)} %pad_clamp_fusion), kind=kCustom, calls=%fused_computation | custom fusion | bytes 792576 | tf_op jit(solution)/shard_map/gather | solution.py:106
  59.2 0.3 broadcast_select_fusion
  59.5 28.7 %all_to_all.27 = bf16[32,48,128]{2,1,0:T(8,128)(2,1)} all-to-all(bf16[32,48,128]{2,1,0:T(8,128)(2,1)S(1)} %broadcast_select_fusion), channel_id=1, replica_groups=mesh['sp'=32,'tp'=16] {'sp'}, dimensions={0} | all-to-all | bytes 786432 | tf_op jit(solution)/shard_map/all_to_all | solution.py:109
  88.2 52.3 %all-gather.4.cloned.1.call-done = bf16[1,1536,2048]{2,1,0:T(8,128)(2,1)} async-done(((bf16[1,1536,128]{2,1,0:T(8,128)(2,1)}), bf16[1,1536,2048]{2,1,0:T(8,128)(2,1)}) %all-gather.4.cloned.1.call-update) | async-done | bytes 6291472 | tf_op jit(solution)/shard_map/all_gather | solution.py:110
  140.5 3.4 %copy.70 = bf16[2,32,24,2048]{3,2,1,0:T(8,128)(2,1)S(1)} copy(bf16[2,32,24,2048]{3,2,0,1:T(8,128)(2,1)} %bitcast.62) | data formatting | bytes 12582912 | tf_op jit(solution)/shard_map/transpose | solution.py:113
  143.9 1.8 fusion.20
  145.7 2.5 fusion
  148.3 0.2 all-gather.8.cloned.1.call-start
  148.5 0.5 all-gather.8.cloned.1.call-update
  149.1 0.1 reshape.110
  149.3 58.0 %all-gather.6.cloned.1.call-done = bf16[2,768,2048]{2,1,0:T(8,128)(2,1)} async-done(((bf16[2,768,128]{2,1,0:T(8,128)(2,1)}), bf16[2,768,2048]{2,1,0:T(8,128)(2,1)}) %all-gather.6.cloned.1.call-update) | async-done | bytes 6291472 | tf_op jit(solution)/shard_map/all_gather | solution.py:122
  207.3 4.6 %convolution_convert_fusion = bf16[2,768,128]{2,1,0:T(8,128)(2,1)S(1)} fusion(bf16[2,768,2048]{2,1,0:T(8,128)(2,1)} %all-gather.6.cloned.1.call-done, bf16[2,2048,128]{2,1,0:T(8,128)(2,1)S(1)} %copy-done.7), kind=kOutput, calls=%fused_computation.5 | convolution fusion | flops 805502976 | bytes 7733248 | tf_op jit(solution)/shard_map/erf,efd->erd/dot_general | solution.py:120
  211.9 6.1 %copy.88 = bf16[1,1536,128]{2,0,1:T(2,128)(2,1)S(1)} copy(bf16[1,1536,128]{2,1,0:T(8,128)(2,1)S(1)} %bitcast.67) | data formatting | bytes 786432 | tf_op jit(solution)/shard_map/reshape | solution.py:130
  218.1 0.6 broadcast.89
  218.7 8.8 %reduce.7 = bf16[1536,128]{1,0:T(8,128)(2,1)S(1)} reduce(bf16[1536,1,128]{2,1,0:T(2,128)(2,1)S(1)} %bitcast.63, bf16[]{:T(256)} %broadcast.89), dimensions={1}, to_apply=%bitcast.56.reduce_sub_computation | reduce | bytes 786434
  227.5 0.8 reshape.133
  228.3 9.9 %all-to-all-start.2 = ((bf16[32,2,3072]{2,1,0:T(2,128)(2,1)}), bf16[32,2,3072]{2,1,0:T(2,128)(2,1)S(1)}, u32[]{:S(2)}, u32[]{:S(2)}) async-start(bf16[32,2,3072]{2,1,0:T(2,128)(2,1)} %reshape.133), calls=%async_computation.2 | async-start | bytes 786432 | tf_op jit(solution)/shard_map/all_to_all | solution.py:132
  238.3 0.1 copy.82
  238.4 11.7 %all-gather.8.cloned.1.call-done = bf16[384,2048]{0,1:T(8,128)(2,1)} async-done(((bf16[384,128]{0,1:T(8,128)(2,1)}), bf16[384,2048]{0,1:T(8,128)(2,1)}) %all-gather.8.cloned.1.call-update) | async-done | bytes 1572880 | tf_op jit(solution)/shard_map/all_gather | solution.py:88
  250.1 1.7 fusion.21
  251.9 1.8 fusion.4
  253.7 16.9 %all_gather.19 = bf16[384,512]{0,1:T(8,128)(2,1)S(1)} all-gather(bf16[384,32]{0,1:T(8,128)(2,1)S(1)} %fusion.4), channel_id=1, replica_groups=mesh['sp'=32,'tp'=16] {'tp'}, dimensions={1}, use_global_device_ids=true | all-gather | bytes 417792 | tf_op jit(solution)/shard_map/all_gather | solution.py:95
  270.5 0.3 reshape.134
  270.9 1.9 gather_fusion.1
  272.8 0.6 multiply_reduce_fusion
  273.5 0.3 fusion.3
  273.8 0.8 copy.74
  (45 shorter events, 1.1 us)
Async XLA Ops:
  6.5 137.4 %copy-start = (bf16[2,2048,128]{2,1,0:T(8,128)(2,1)S(1)}, bf16[2,2048,128]{2,1,0:T(8,128)(2,1)}, u32[]{:S(2)}) copy-start(bf16[2,2048,128]{2,1,0:T(8,128)(2,1)} %param.24) | copy-start | bytes 3145732
  7.5 14.2 %collective-permute-start = (bf16[32,1]{1,0:T(8,128)(2,1)S(1)}, bf16[32,1]{1,0:T(8,128)(2,1)S(1)}, u32[]{:S(2)}, u32[]{:S(2)}) collective-permute-start(bf16[32,1]{1,0:T(8,128)(2,1)S(1)} %get-tuple-element.7), channel_id=1, source_target_pairs={{0,16},{16,32},{32,48},{48,64},{64,80},{80,96},{96,112},{112,128},... | collective-permute-start | bytes 200 | tf_op jit(solution)/shard_map/ppermute | solution.py:18
  11.4 10.2 %collective-permute-start.1 = (bf16[32,1]{1,0:T(8,128)(2,1)S(1)}, bf16[32,1]{1,0:T(8,128)(2,1)S(1)}, u32[]{:S(2)}, u32[]{:S(2)}) collective-permute-start(bf16[32,1]{1,0:T(8,128)(2,1)S(1)} %get-tuple-element.8), channel_id=1, source_target_pairs={{16,0},{32,16},{48,32},{64,48},{80,64},{96,80},{112,96},{128,112},... | collective-permute-start | bytes 200 | tf_op jit(solution)/shard_map/ppermute | solution.py:19
  43.9 11.9 %all-to-all-start = ((f32[16,1,384]{2,1,0:T(1,128)}), f32[16,1,384]{2,1,0:T(1,128)S(1)}, u32[]{:S(2)}, u32[]{:S(2)}) async-start(f32[16,1,384]{2,1,0:T(1,128)} %broadcast_in_dim.38), calls=%async_computation | async-start | bytes 49152 | tf_op jit(solution)/shard_map/all_to_all | solution.py:26
  48.3 92.2 %all-gather.4.cloned.1.call-start = ((), (), s32[]{:S(2)}) async-start(), calls=%async_computation.3 | async-start | bytes 6684672 | tf_op jit(solution)/shard_map/all_gather | solution.py:110
  55.9 88.0 %copy-start.1 = (bf16[384,128]{0,1:T(8,128)(2,1)}, bf16[384,128]{0,1:T(8,128)(2,1)S(1)}, u32[]{:S(2)}) copy-start(bf16[384,128]{0,1:T(8,128)(2,1)S(1)} %multiply_convert_fusion) | copy-start | bytes 294916
  88.2 119.1 %all-gather.6.cloned.1.call-start = ((), (), s32[]{:S(2)}) async-start(), calls=%async_computation.4 | async-start | bytes 6684672 | tf_op jit(solution)/shard_map/all_gather | solution.py:122
  143.9 1.8 copy-start.6
  145.7 3.3 %copy-start.5 = (f32[384,2]{0,1:T(2,128)S(1)}, f32[384,2]{0,1:T(2,128)}, u32[]{:S(2)}) copy-start(f32[384,2]{0,1:T(2,128)} %param.23) | copy-start | bytes 9220
  145.7 61.6 %copy-start.7 = (bf16[2,2048,128]{2,1,0:T(8,128)(2,1)S(1)}, bf16[2,2048,128]{2,1,0:T(8,128)(2,1)}, u32[]{:S(2)}) copy-start(bf16[2,2048,128]{2,1,0:T(8,128)(2,1)} %param.26) | copy-start | bytes 3145732
  148.3 101.8 %all-gather.8.cloned.1.call-start = ((), (), s32[]{:S(2)}) async-start(), calls=%async_computation.5 | async-start | bytes 1671168 | tf_op jit(solution)/shard_map/all_gather | solution.py:88
  149.2 100.9 %copy-start.3 = (bf16[2048,32]{0,1:T(8,128)(2,1)S(1)}, bf16[2048,32]{0,1:T(8,128)(2,1)}, u32[]{:S(2)}) copy-start(bf16[2048,32]{0,1:T(8,128)(2,1)} %param.27) | copy-start | bytes 393220
  149.3 102.6 %copy-start.2 = (bf16[2048,32]{0,1:T(8,128)(2,1)S(1)}, bf16[2048,32]{0,1:T(8,128)(2,1)}, u32[]{:S(2)}) copy-start(bf16[2048,32]{0,1:T(8,128)(2,1)} %param.28) | copy-start | bytes 393220
  218.1 55.5 %copy-start.4 = (bf16[512,128]{1,0:T(8,128)(2,1)S(1)}, bf16[512,128]{1,0:T(8,128)(2,1)}, u32[]{:S(2)}) copy-start(bf16[512,128]{1,0:T(8,128)(2,1)} %param.29) | copy-start | bytes 393220
  228.3 42.2 %all-to-all-start.2 = ((bf16[32,2,3072]{2,1,0:T(2,128)(2,1)}), bf16[32,2,3072]{2,1,0:T(2,128)(2,1)S(1)}, u32[]{:S(2)}, u32[]{:S(2)}) async-start(bf16[32,2,3072]{2,1,0:T(2,128)(2,1)} %reshape.133), calls=%async_computation.2 | async-start | bytes 786432 | tf_op jit(solution)/shard_map/all_to_all | solution.py:132
Sparse Core Ops, SparseCore 0:
  88.3 52.1 all-gather.3
  148.4 58.8 all-gather.5
  209.4 40.6 all-gather.7
where the time goes:
time: 282 us; the launch traced here: 281 us
  waiting for transfers between devices  129 us (46%)
  blocking collectives  65 us (23%)
  local copies, waits for them, and re-layouts  24.6 us (9%)
  starting transfers between devices  19.9 us (7%)
  other arithmetic  15 us (5%)
  matrix products  13.9 us (5%)
  between operations  13.5 us (5%)
    all_gather x1, waiting for transfers between devices, local(): lax.all_gather(hidden, 'tp', axis=2, tiled=True)  58 us
    all_gather x1, waiting for transfers between devices, local(): received = lax.all_gather(sliced, 'tp', axis=2, tiled=True)  52.3 us
    all_to_all x1, blocking collectives, local(): lax.all_to_all(outgoing, 'sp', split_axis=0, concat_axis=1, tiled=True)  28.7 us
    all_gather x1, blocking collectives, local(): lax.all_gather(mixed, 'tp', axis=0, tiled=True)  19.5 us
    all_gather x1, blocking collectives, local(): lax.all_gather(shared_act, 'tp', axis=1, tiled=True)  16.9 us
    all_gather x1, waiting for transfers between devices, local(): whole_rows = lax.all_gather(normed, 'tp', axis=1, tiled=True)  11.7 us
    all_to_all x1, starting transfers between devices, local(): lax.all_to_all(regrouped, 'sp', split_axis=1, concat_axis=0, tiled=True)  9.9 us
    unnamed x2, other arithmetic  9.43 us
  transfers between devices with their start and end apart: 7, of which 4 were waited for; matrix products, arithmetic and copies ran while one was open for 12% of the time, Pallas kernels for 0%

commit v1 on v0

--- a/solution.py
+++ b/solution.py
@@ -6,6 +6,24 @@
 D = 2048
 epsilon = 1e-06
 routed_scale = 2.5
+
+
+def gather_around(shard, axis, dim):
+    ways, here, turn = (lax.axis_size(axis), lax.axis_index(axis), shard.shape[dim])
+    shape = [n * ways if d == dim else n for d, n in enumerate(shard.shape)]
+    full = lax.dynamic_update_slice_in_dim(
+        jnp.zeros(shape, shard.dtype), shard, here * turn, axis=dim
+    )
+    going_up = going_down = shard
+    for far in range(1, ways // 2 + 1):
+        going_up = lax.ppermute(going_up, axis, [(d, (d + 1) % ways) for d in range(ways)])
+        full = lax.dynamic_update_slice_in_dim(full, going_up, (here - far) % ways * turn, axis=dim)
+        if 2 * far < ways:
+            going_down = lax.ppermute(going_down, axis, [(d, (d - 1) % ways) for d in range(ways)])
+            full = lax.dynamic_update_slice_in_dim(
+                full, going_down, (here + far) % ways * turn, axis=dim
+            )
+    return full
 
 
 def extended(array, sides, width):
@@ -75,7 +93,7 @@
     token_count = mixed.shape[1]
     rows_w = mix_weight
     projected = lax.dot_general(
-        lax.all_gather(mixed, "tp", axis=0, tiled=True),
+        gather_around(mixed, "tp", 0),
         rows_w,
         (((0,), (0,)), ((), ())),
         preferred_element_type=jnp.float32,

time: 282 us -> 301 us (1.067)
  starting transfers between devices: 19.9 us -> 48.7 us
  blocking collectives: 65 us -> 45.5 us
  waiting for transfers between devices: 129 us -> 138 us
    ppermute x0 -> x15, starting transfers between devices: none -> 25.7 us  [the longest x7 23.4 us: gather_around(): lax.ppermute(going_down, axis, [(d, (d - 1) % ways) for d in range(ways)])]
    all_gather x1 -> x0, blocking collectives: 19.5 us -> none  [local(): lax.all_gather(mixed, 'tp', axis=0, tiled=True)]
    ppermute x0 -> x15, waiting for transfers between devices: none -> 9.22 us  [the longest x8 8.18 us: gather_around(): lax.ppermute(going_up, axis, [(d, (d + 1) % ways) for d in range(ways)])]
    all_to_all x1, starting transfers between devices: 4.49 us -> 7.64 us  [copy_for_each(): lax.all_to_all(jnp.broadcast_to(array[None], (peers, *array.shape)), axis...]
  transfers between devices with their start and end apart: 7 -> 22, of which waited for: 4 -> 17; matrix products, arithmetic and copies ran while one was open for 12% -> 11% of each run, Pallas kernels for 0% -> 0%
where the time goes in v1:
time: 301 us; the launch traced here: 300 us
  waiting for transfers between devices  138 us (46%)
  starting transfers between devices  48.7 us (16%)
  blocking collectives  45.5 us (15%)
  local copies, waits for them, and re-layouts  24.8 us (8%)
  other arithmetic  15 us (5%)
  matrix products  13.9 us (5%)
  between operations  13.6 us (5%)
    all_gather x1, waiting for transfers between devices, local(): lax.all_gather(hidden, 'tp', axis=2, tiled=True)  58 us
    all_gather x1, waiting for transfers between devices, local(): received = lax.all_gather(sliced, 'tp', axis=2, tiled=True)  52.3 us
    all_to_all x1, blocking collectives, local(): lax.all_to_all(outgoing, 'sp', split_axis=0, concat_axis=1, tiled=True)  28.7 us
    ppermute x7, starting transfers between devices, gather_around(): lax.ppermute(going_down, axis, [(d, (d - 1) % ways) for d in range(ways)])  23.4 us
    all_gather x1, blocking collectives, local(): lax.all_gather(shared_act, 'tp', axis=1, tiled=True)  16.9 us
    all_gather x1, waiting for transfers between devices, local(): whole_rows = lax.all_gather(normed, 'tp', axis=1, tiled=True)  11.8 us
    all_to_all x1, starting transfers between devices, local(): lax.all_to_all(regrouped, 'sp', split_axis=1, concat_axis=0, tiled=True)  9.9 us
    unnamed x2, other arithmetic  9.37 us
  transfers between devices with their start and end apart: 22, of which 17 were waited for; matrix products, arithmetic and copies ran while one was open for 11% of the time, Pallas kernels for 0%

profile of v1, /device:TPU:1, one launch (start us, length us, event | category | flops | bytes accessed | tf_op | source)
XLA Modules:
  0.0 300.1 jit_solution(16814710883520530095)
XLA Ops:
  6.5 0.9 multiply_convert_fusion.1
  7.5 3.9 %collective-permute-start = (bf16[32,1]{1,0:T(8,128)(2,1)S(1)}, bf16[32,1]{1,0:T(8,128)(2,1)S(1)}, u32[]{:S(2)}, u32[]{:S(2)}) collective-permute-start(bf16[32,1]{1,0:T(8,128)(2,1)S(1)} %get-tuple-element.9), channel_id=1, source_target_pairs={{0,16},{16,32},{32,48},{48,64},{64,80},{80,96},{96,112},{112,128},... | collective-permute-start | bytes 200 | tf_op jit(solution)/shard_map/ppermute | solution.py:36
  11.4 1.3 collective-permute-start.1
  12.7 0.8 copy.64
  13.8 0.7 convert_element_type.58
  14.5 1.8 reduce-window.6
  17.2 3.4 %scatter_custom_fusion = s32[1536]{0:T(1024)S(1)} fusion(s32[768]{0:T(1024)S(1)} %fusion.18, s32[768]{0:T(1024)S(1)} %add_select_fusion, s32[]{:T(128)} %constant.129.clone.1), kind=kCustom, calls=%fused_computation.49 | custom fusion | bytes 6148 | tf_op jit(solution)/shard_map/scatter | solution.py:63
  20.8 0.9 constant_dynamic-update-slice_fusion.15
  21.6 2.1 collective-permute-start.2
  23.8 2.1 collective-permute-start.3
  25.9 1.0 copy.63
  27.0 3.3 %collective-permute-start.5 = (bf16[32,384]{1,0:T(8,128)(2,1)S(1)}, bf16[32,384]{1,0:T(8,128)(2,1)S(1)}, u32[]{:S(2)}, u32[]{:S(2)}) collective-permute-start(bf16[32,384]{1,0:T(8,128)(2,1)S(1)} %collective-permute-done.3), channel_id=1, source_target_pairs={{0,15},{1,0},{2,1},{3,2},{4,3},{5,4},{6,5},{7,6},{8,7},{9,8},{10,9... | collective-permute-start | bytes 73736 | tf_op jit(solution)/shard_map/ppermute | solution.py:22
  30.3 0.7 collective-permute-done.4
  31.2 3.6 %collective-permute-start.7 = (bf16[32,384]{1,0:T(8,128)(2,1)S(1)}, bf16[32,384]{1,0:T(8,128)(2,1)S(1)}, u32[]{:S(2)}, u32[]{:S(2)}) collective-permute-start(bf16[32,384]{1,0:T(8,128)(2,1)S(1)} %collective-permute-done.5), channel_id=1, source_target_pairs={{0,15},{1,0},{2,1},{3,2},{4,3},{5,4},{6,5},{7,6},{8,7},{9,8},{10,9... | collective-permute-start | bytes 73736 | tf_op jit(solution)/shard_map/ppermute | solution.py:22
  34.8 0.6 collective-permute-done.6
  35.6 3.6 %collective-permute-start.9 = (bf16[32,384]{1,0:T(8,128)(2,1)S(1)}, bf16[32,384]{1,0:T(8,128)(2,1)S(1)}, u32[]{:S(2)}, u32[]{:S(2)}) collective-permute-start(bf16[32,384]{1,0:T(8,128)(2,1)S(1)} %collective-permute-done.7), channel_id=1, source_target_pairs={{0,15},{1,0},{2,1},{3,2},{4,3},{5,4},{6,5},{7,6},{8,7},{9,8},{10,9... | collective-permute-start | bytes 73736 | tf_op jit(solution)/shard_map/ppermute | solution.py:22
  39.3 0.6 collective-permute-done.8
  40.1 3.6 %collective-permute-start.11 = (bf16[32,384]{1,0:T(8,128)(2,1)S(1)}, bf16[32,384]{1,0:T(8,128)(2,1)S(1)}, u32[]{:S(2)}, u32[]{:S(2)}) collective-permute-start(bf16[32,384]{1,0:T(8,128)(2,1)S(1)} %collective-permute-done.9), channel_id=1, source_target_pairs={{0,15},{1,0},{2,1},{3,2},{4,3},{5,4},{6,5},{7,6},{8,7},{9,8},{10,9... | collective-permute-start | bytes 73736 | tf_op jit(solution)/shard_map/ppermute | solution.py:22
  43.7 0.6 collective-permute-done.10
  44.5 3.6 %collective-permute-start.13 = (bf16[32,384]{1,0:T(8,128)(2,1)S(1)}, bf16[32,384]{1,0:T(8,128)(2,1)S(1)}, u32[]{:S(2)}, u32[]{:S(2)}) collective-permute-start(bf16[32,384]{1,0:T(8,128)(2,1)S(1)} %collective-permute-done.11), channel_id=1, source_target_pairs={{0,15},{1,0},{2,1},{3,2},{4,3},{5,4},{6,5},{7,6},{8,7},{9,8},{10,9... | collective-permute-start | bytes 73736 | tf_op jit(solution)/shard_map/ppermute | solution.py:22
  48.2 0.6 collective-permute-done.12
  49.0 3.6 %collective-permute-start.15 = (bf16[32,384]{1,0:T(8,128)(2,1)S(1)}, bf16[32,384]{1,0:T(8,128)(2,1)S(1)}, u32[]{:S(2)}, u32[]{:S(2)}) collective-permute-start(bf16[32,384]{1,0:T(8,128)(2,1)S(1)} %collective-permute-done.13), channel_id=1, source_target_pairs={{0,15},{1,0},{2,1},{3,2},{4,3},{5,4},{6,5},{7,6},{8,7},{9,8},{10,9... | collective-permute-start | bytes 73736 | tf_op jit(solution)/shard_map/ppermute | solution.py:22
  52.6 0.6 collective-permute-done.14
  53.5 4.3 %collective-permute-done.16 = bf16[32,384]{1,0:T(8,128)(2,1)S(1)} collective-permute-done((bf16[32,384]{1,0:T(8,128)(2,1)S(1)}, bf16[32,384]{1,0:T(8,128)(2,1)S(1)}, u32[]{:S(2)}, u32[]{:S(2)}) %collective-permute-start.16) | collective-permute-done | bytes 24608 | tf_op jit(solution)/shard_map/ppermute | solution.py:19
  57.8 1.2 multiply_reduce_fusion.1
  59.0 0.6 broadcast_in_dim.42
  59.6 7.6 %all-to-all-start = ((f32[16,1,384]{2,1,0:T(1,128)}), f32[16,1,384]{2,1,0:T(1,128)S(1)}, u32[]{:S(2)}, u32[]{:S(2)}) async-start(f32[16,1,384]{2,1,0:T(1,128)} %broadcast_in_dim.42), calls=%async_computation | async-start | bytes 49152 | tf_op jit(solution)/shard_map/all_to_all | solution.py:44
  67.3 0.7 convert_element_type.68
  68.0 6.6 %all-to-all-done = f32[16,1,384]{2,1,0:T(1,128)S(1)} async-done(((f32[16,1,384]{2,1,0:T(1,128)}), f32[16,1,384]{2,1,0:T(1,128)S(1)}, u32[]{:S(2)}, u32[]{:S(2)}) %all-to-all-start) | async-done | bytes 24608 | tf_op jit(solution)/shard_map/all_to_all | solution.py:44
  74.9 3.2 %gather_fusion = bf16[1536,128]{1,0:T(8,128)(2,1)S(1)} fusion(bf16[384,128]{1,0:T(8,128)(2,1)S(1)} %copy.69, s32[2048]{0:T(1024)S(1)} %pad_clamp_fusion), kind=kCustom, calls=%fused_computation | custom fusion | bytes 792576 | tf_op jit(solution)/shard_map/gather | solution.py:124
  78.4 28.7 %all_to_all.27 = bf16[32,48,128]{2,1,0:T(8,128)(2,1)} all-to-all(bf16[32,48,128]{2,1,0:T(8,128)(2,1)S(1)} %broadcast_select_fusion), channel_id=1, replica_groups=mesh['sp'=32,'tp'=16] {'sp'}, dimensions={0} | all-to-all | bytes 786432 | tf_op jit(solution)/shard_map/all_to_all | solution.py:127
  107.1 52.3 %all-gather.4.cloned.1.call-done = bf16[1,1536,2048]{2,1,0:T(8,128)(2,1)} async-done(((bf16[1,1536,128]{2,1,0:T(8,128)(2,1)}), bf16[1,1536,2048]{2,1,0:T(8,128)(2,1)}) %all-gather.4.cloned.1.call-update) | async-done | bytes 6291472 | tf_op jit(solution)/shard_map/all_gather | solution.py:128
  159.4 3.4 %copy.70 = bf16[2,32,24,2048]{3,2,1,0:T(8,128)(2,1)S(1)} copy(bf16[2,32,24,2048]{3,2,0,1:T(8,128)(2,1)} %bitcast.62) | data formatting | bytes 12582912 | tf_op jit(solution)/shard_map/transpose | solution.py:131
  162.8 1.8 fusion.21
  164.7 2.6 fusion
  168.2 58.0 %all-gather.6.cloned.1.call-done = bf16[2,768,2048]{2,1,0:T(8,128)(2,1)} async-done(((bf16[2,768,128]{2,1,0:T(8,128)(2,1)}), bf16[2,768,2048]{2,1,0:T(8,128)(2,1)}) %all-gather.6.cloned.1.call-update) | async-done | bytes 6291472 | tf_op jit(solution)/shard_map/all_gather | solution.py:140
  226.3 4.6 %convolution_convert_fusion = bf16[2,768,128]{2,1,0:T(8,128)(2,1)S(1)} fusion(bf16[2,768,2048]{2,1,0:T(8,128)(2,1)} %all-gather.6.cloned.1.call-done, bf16[2,2048,128]{2,1,0:T(8,128)(2,1)S(1)} %copy-done.7), kind=kOutput, calls=%fused_computation.5 | convolution fusion | flops 805502976 | bytes 7733248 | tf_op jit(solution)/shard_map/erf,efd->erd/dot_general | solution.py:138
  230.9 6.1 %copy.88 = bf16[1,1536,128]{2,0,1:T(2,128)(2,1)S(1)} copy(bf16[1,1536,128]{2,1,0:T(8,128)(2,1)S(1)} %bitcast.67) | data formatting | bytes 786432 | tf_op jit(solution)/shard_map/reshape | solution.py:148
  237.6 8.8 %reduce.7 = bf16[1536,128]{1,0:T(8,128)(2,1)S(1)} reduce(bf16[1536,1,128]{2,1,0:T(2,128)(2,1)S(1)} %bitcast.63, bf16[]{:T(256)} %broadcast.108), dimensions={1}, to_apply=%bitcast.56.reduce_sub_computation | reduce | bytes 786434
  246.4 0.8 reshape.133
  247.2 9.9 %all-to-all-start.2 = ((bf16[32,2,3072]{2,1,0:T(2,128)(2,1)}), bf16[32,2,3072]{2,1,0:T(2,128)(2,1)S(1)}, u32[]{:S(2)}, u32[]{:S(2)}) async-start(bf16[32,2,3072]{2,1,0:T(2,128)(2,1)} %reshape.133), calls=%async_computation.2 | async-start | bytes 786432 | tf_op jit(solution)/shard_map/all_to_all | solution.py:150
  257.3 11.8 %all-gather.8.cloned.1.call-done = bf16[384,2048]{0,1:T(8,128)(2,1)} async-done(((bf16[384,128]{0,1:T(8,128)(2,1)}), bf16[384,2048]{0,1:T(8,128)(2,1)}) %all-gather.8.cloned.1.call-update) | async-done | bytes 1572880 | tf_op jit(solution)/shard_map/all_gather | solution.py:106
  269.1 1.7 fusion.22
  270.9 1.8 fusion.4
  272.6 16.9 %all_gather.15 = bf16[384,512]{0,1:T(8,128)(2,1)S(1)} all-gather(bf16[384,32]{0,1:T(8,128)(2,1)S(1)} %fusion.4), channel_id=1, replica_groups=mesh['sp'=32,'tp'=16] {'tp'}, dimensions={1}, use_global_device_ids=true | all-gather | bytes 417792 | tf_op jit(solution)/shard_map/all_gather | solution.py:113
  289.9 1.9 gather_fusion.1
  291.8 0.6 multiply_reduce_fusion
  292.8 0.8 copy.74
  (90 shorter events, 5.8 us)
Async XLA Ops:
  6.5 156.3 %copy-start = (bf16[2,2048,128]{2,1,0:T(8,128)(2,1)S(1)}, bf16[2,2048,128]{2,1,0:T(8,128)(2,1)}, u32[]{:S(2)}) copy-start(bf16[2,2048,128]{2,1,0:T(8,128)(2,1)} %param.24) | copy-start | bytes 3145732
  7.5 13.1 %collective-permute-start = (bf16[32,1]{1,0:T(8,128)(2,1)S(1)}, bf16[32,1]{1,0:T(8,128)(2,1)S(1)}, u32[]{:S(2)}, u32[]{:S(2)}) collective-permute-start(bf16[32,1]{1,0:T(8,128)(2,1)S(1)} %get-tuple-element.9), channel_id=1, source_target_pairs={{0,16},{16,32},{32,48},{48,64},{64,80},{80,96},{96,112},{112,128},... | collective-permute-start | bytes 200 | tf_op jit(solution)/shard_map/ppermute | solution.py:36
  11.4 9.2 %collective-permute-start.1 = (bf16[32,1]{1,0:T(8,128)(2,1)S(1)}, bf16[32,1]{1,0:T(8,128)(2,1)S(1)}, u32[]{:S(2)}, u32[]{:S(2)}) collective-permute-start(bf16[32,1]{1,0:T(8,128)(2,1)S(1)} %get-tuple-element.10), channel_id=1, source_target_pairs={{16,0},{32,16},{48,32},{64,48},{80,64},{96,80},{112,96},{128,112},... | collective-permute-start | bytes 200 | tf_op jit(solution)/shard_map/ppermute | solution.py:37
  21.6 5.3 %collective-permute-start.2 = (bf16[32,384]{1,0:T(8,128)(2,1)S(1)}, bf16[32,384]{1,0:T(8,128)(2,1)S(1)}, u32[]{:S(2)}, u32[]{:S(2)}) collective-permute-start(bf16[32,384]{1,0:T(8,128)(2,1)S(1)} %get-tuple-element.6), channel_id=1, source_target_pairs={{0,1},{1,2},{2,3},{3,4},{4,5},{5,6},{6,7},{7,8},{8,9},{9,10},{10,1... | collective-permute-start | bytes 73736 | tf_op jit(solution)/shard_map/ppermute | solution.py:19
  23.8 3.3 %collective-permute-start.3 = (bf16[32,384]{1,0:T(8,128)(2,1)S(1)}, bf16[32,384]{1,0:T(8,128)(2,1)S(1)}, u32[]{:S(2)}, u32[]{:S(2)}) collective-permute-start(bf16[32,384]{1,0:T(8,128)(2,1)S(1)} %get-tuple-element.6), channel_id=1, source_target_pairs={{0,15},{1,0},{2,1},{3,2},{4,3},{5,4},{6,5},{7,6},{8,7},{9,8},{10,9... | collective-permute-start | bytes 73736 | tf_op jit(solution)/shard_map/ppermute | solution.py:22
  27.0 4.0 %collective-permute-start.4 = (bf16[32,384]{1,0:T(8,128)(2,1)S(1)}, bf16[32,384]{1,0:T(8,128)(2,1)S(1)}, u32[]{:S(2)}, u32[]{:S(2)}) collective-permute-start(bf16[32,384]{1,0:T(8,128)(2,1)S(1)} %collective-permute-done.2), channel_id=1, source_target_pairs={{0,1},{1,2},{2,3},{3,4},{4,5},{5,6},{6,7},{7,8},{8,9},{9,10},{10,1... | collective-permute-start | bytes 73736 | tf_op jit(solution)/shard_map/ppermute | solution.py:19
  27.0 4.1 %collective-permute-start.5 = (bf16[32,384]{1,0:T(8,128)(2,1)S(1)}, bf16[32,384]{1,0:T(8,128)(2,1)S(1)}, u32[]{:S(2)}, u32[]{:S(2)}) collective-permute-start(bf16[32,384]{1,0:T(8,128)(2,1)S(1)} %collective-permute-done.3), channel_id=1, source_target_pairs={{0,15},{1,0},{2,1},{3,2},{4,3},{5,4},{6,5},{7,6},{8,7},{9,8},{10,9... | collective-permute-start | bytes 73736 | tf_op jit(solution)/shard_map/ppermute | solution.py:22
  31.0 4.5 %collective-permute-start.6 = (bf16[32,384]{1,0:T(8,128)(2,1)S(1)}, bf16[32,384]{1,0:T(8,128)(2,1)S(1)}, u32[]{:S(2)}, u32[]{:S(2)}) collective-permute-start(bf16[32,384]{1,0:T(8,128)(2,1)S(1)} %collective-permute-done.4), channel_id=1, source_target_pairs={{0,1},{1,2},{2,3},{3,4},{4,5},{5,6},{6,7},{7,8},{8,9},{9,10},{10,1... | collective-permute-start | bytes 73736 | tf_op jit(solution)/shard_map/ppermute | solution.py:19
  31.2 4.5 %collective-permute-start.7 = (bf16[32,384]{1,0:T(8,128)(2,1)S(1)}, bf16[32,384]{1,0:T(8,128)(2,1)S(1)}, u32[]{:S(2)}, u32[]{:S(2)}) collective-permute-start(bf16[32,384]{1,0:T(8,128)(2,1)S(1)} %collective-permute-done.5), channel_id=1, source_target_pairs={{0,15},{1,0},{2,1},{3,2},{4,3},{5,4},{6,5},{7,6},{8,7},{9,8},{10,9... | collective-permute-start | bytes 73736 | tf_op jit(solution)/shard_map/ppermute | solution.py:22
  35.4 4.5 %collective-permute-start.8 = (bf16[32,384]{1,0:T(8,128)(2,1)S(1)}, bf16[32,384]{1,0:T(8,128)(2,1)S(1)}, u32[]{:S(2)}, u32[]{:S(2)}) collective-permute-start(bf16[32,384]{1,0:T(8,128)(2,1)S(1)} %collective-permute-done.6), channel_id=1, source_target_pairs={{0,1},{1,2},{2,3},{3,4},{4,5},{5,6},{6,7},{7,8},{8,9},{9,10},{10,1... | collective-permute-start | bytes 73736 | tf_op jit(solution)/shard_map/ppermute | solution.py:19
  35.6 4.5 %collective-permute-start.9 = (bf16[32,384]{1,0:T(8,128)(2,1)S(1)}, bf16[32,384]{1,0:T(8,128)(2,1)S(1)}, u32[]{:S(2)}, u32[]{:S(2)}) collective-permute-start(bf16[32,384]{1,0:T(8,128)(2,1)S(1)} %collective-permute-done.7), channel_id=1, source_target_pairs={{0,15},{1,0},{2,1},{3,2},{4,3},{5,4},{6,5},{7,6},{8,7},{9,8},{10,9... | collective-permute-start | bytes 73736 | tf_op jit(solution)/shard_map/ppermute | solution.py:22
  39.9 4.5 %collective-permute-start.10 = (bf16[32,384]{1,0:T(8,128)(2,1)S(1)}, bf16[32,384]{1,0:T(8,128)(2,1)S(1)}, u32[]{:S(2)}, u32[]{:S(2)}) collective-permute-start(bf16[32,384]{1,0:T(8,128)(2,1)S(1)} %collective-permute-done.8), channel_id=1, source_target_pairs={{0,1},{1,2},{2,3},{3,4},{4,5},{5,6},{6,7},{7,8},{8,9},{9,10},{10,1... | collective-permute-start | bytes 73736 | tf_op jit(solution)/shard_map/ppermute | solution.py:19
  40.1 4.5 %collective-permute-start.11 = (bf16[32,384]{1,0:T(8,128)(2,1)S(1)}, bf16[32,384]{1,0:T(8,128)(2,1)S(1)}, u32[]{:S(2)}, u32[]{:S(2)}) collective-permute-start(bf16[32,384]{1,0:T(8,128)(2,1)S(1)} %collective-permute-done.9), channel_id=1, source_target_pairs={{0,15},{1,0},{2,1},{3,2},{4,3},{5,4},{6,5},{7,6},{8,7},{9,8},{10,9... | collective-permute-start | bytes 73736 | tf_op jit(solution)/shard_map/ppermute | solution.py:22
  44.4 4.5 %collective-permute-start.12 = (bf16[32,384]{1,0:T(8,128)(2,1)S(1)}, bf16[32,384]{1,0:T(8,128)(2,1)S(1)}, u32[]{:S(2)}, u32[]{:S(2)}) collective-permute-start(bf16[32,384]{1,0:T(8,128)(2,1)S(1)} %collective-permute-done.10), channel_id=1, source_target_pairs={{0,1},{1,2},{2,3},{3,4},{4,5},{5,6},{6,7},{7,8},{8,9},{9,10},{10,1... | collective-permute-start | bytes 73736 | tf_op jit(solution)/shard_map/ppermute | solution.py:19
  44.5 4.5 %collective-permute-start.13 = (bf16[32,384]{1,0:T(8,128)(2,1)S(1)}, bf16[32,384]{1,0:T(8,128)(2,1)S(1)}, u32[]{:S(2)}, u32[]{:S(2)}) collective-permute-start(bf16[32,384]{1,0:T(8,128)(2,1)S(1)} %collective-permute-done.11), channel_id=1, source_target_pairs={{0,15},{1,0},{2,1},{3,2},{4,3},{5,4},{6,5},{7,6},{8,7},{9,8},{10,9... | collective-permute-start | bytes 73736 | tf_op jit(solution)/shard_map/ppermute | solution.py:22
  48.8 4.5 %collective-permute-start.14 = (bf16[32,384]{1,0:T(8,128)(2,1)S(1)}, bf16[32,384]{1,0:T(8,128)(2,1)S(1)}, u32[]{:S(2)}, u32[]{:S(2)}) collective-permute-start(bf16[32,384]{1,0:T(8,128)(2,1)S(1)} %collective-permute-done.12), channel_id=1, source_target_pairs={{0,1},{1,2},{2,3},{3,4},{4,5},{5,6},{6,7},{7,8},{8,9},{9,10},{10,1... | collective-permute-start | bytes 73736 | tf_op jit(solution)/shard_map/ppermute | solution.py:19
  49.0 4.5 %collective-permute-start.15 = (bf16[32,384]{1,0:T(8,128)(2,1)S(1)}, bf16[32,384]{1,0:T(8,128)(2,1)S(1)}, u32[]{:S(2)}, u32[]{:S(2)}) collective-permute-start(bf16[32,384]{1,0:T(8,128)(2,1)S(1)} %collective-permute-done.13), channel_id=1, source_target_pairs={{0,15},{1,0},{2,1},{3,2},{4,3},{5,4},{6,5},{7,6},{8,7},{9,8},{10,9... | collective-permute-start | bytes 73736 | tf_op jit(solution)/shard_map/ppermute | solution.py:22
  53.3 4.5 %collective-permute-start.16 = (bf16[32,384]{1,0:T(8,128)(2,1)S(1)}, bf16[32,384]{1,0:T(8,128)(2,1)S(1)}, u32[]{:S(2)}, u32[]{:S(2)}) collective-permute-start(bf16[32,384]{1,0:T(8,128)(2,1)S(1)} %collective-permute-done.14), channel_id=1, source_target_pairs={{0,1},{1,2},{2,3},{3,4},{4,5},{5,6},{6,7},{7,8},{8,9},{9,10},{10,1... | collective-permute-start | bytes 73736 | tf_op jit(solution)/shard_map/ppermute | solution.py:19
  59.6 15.0 %all-to-all-start = ((f32[16,1,384]{2,1,0:T(1,128)}), f32[16,1,384]{2,1,0:T(1,128)S(1)}, u32[]{:S(2)}, u32[]{:S(2)}) async-start(f32[16,1,384]{2,1,0:T(1,128)} %broadcast_in_dim.42), calls=%async_computation | async-start | bytes 49152 | tf_op jit(solution)/shard_map/all_to_all | solution.py:44
  67.2 92.2 %all-gather.4.cloned.1.call-start = ((), (), s32[]{:S(2)}) async-start(), calls=%async_computation.3 | async-start | bytes 6684672 | tf_op jit(solution)/shard_map/all_gather | solution.py:128
  74.8 88.0 %copy-start.1 = (bf16[384,128]{0,1:T(8,128)(2,1)}, bf16[384,128]{0,1:T(8,128)(2,1)S(1)}, u32[]{:S(2)}) copy-start(bf16[384,128]{0,1:T(8,128)(2,1)S(1)} %multiply_convert_fusion) | copy-start | bytes 294916
  107.1 119.2 %all-gather.6.cloned.1.call-start = ((), (), s32[]{:S(2)}) async-start(), calls=%async_computation.4 | async-start | bytes 6684672 | tf_op jit(solution)/shard_map/all_gather | solution.py:140
  162.8 1.8 copy-start.6
  164.6 3.4 %copy-start.5 = (f32[384,2]{0,1:T(2,128)S(1)}, f32[384,2]{0,1:T(2,128)}, u32[]{:S(2)}) copy-start(f32[384,2]{0,1:T(2,128)} %param.23) | copy-start | bytes 9220
  164.6 61.6 %copy-start.7 = (bf16[2,2048,128]{2,1,0:T(8,128)(2,1)S(1)}, bf16[2,2048,128]{2,1,0:T(8,128)(2,1)}, u32[]{:S(2)}) copy-start(bf16[2,2048,128]{2,1,0:T(8,128)(2,1)} %param.26) | copy-start | bytes 3145732
  167.3 101.8 %all-gather.8.cloned.1.call-start = ((), (), s32[]{:S(2)}) async-start(), calls=%async_computation.5 | async-start | bytes 1671168 | tf_op jit(solution)/shard_map/all_gather | solution.py:106
  168.2 100.9 %copy-start.3 = (bf16[2048,32]{0,1:T(8,128)(2,1)S(1)}, bf16[2048,32]{0,1:T(8,128)(2,1)}, u32[]{:S(2)}) copy-start(bf16[2048,32]{0,1:T(8,128)(2,1)} %param.27) | copy-start | bytes 393220
  168.2 102.6 %copy-start.2 = (bf16[2048,32]{0,1:T(8,128)(2,1)S(1)}, bf16[2048,32]{0,1:T(8,128)(2,1)}, u32[]{:S(2)}) copy-start(bf16[2048,32]{0,1:T(8,128)(2,1)} %param.28) | copy-start | bytes 393220
  237.0 55.5 %copy-start.4 = (bf16[512,128]{1,0:T(8,128)(2,1)S(1)}, bf16[512,128]{1,0:T(8,128)(2,1)}, u32[]{:S(2)}) copy-start(bf16[512,128]{1,0:T(8,128)(2,1)} %param.29) | copy-start | bytes 393220
  247.2 42.3 %all-to-all-start.2 = ((bf16[32,2,3072]{2,1,0:T(2,128)(2,1)}), bf16[32,2,3072]{2,1,0:T(2,128)(2,1)S(1)}, u32[]{:S(2)}, u32[]{:S(2)}) async-start(bf16[32,2,3072]{2,1,0:T(2,128)(2,1)} %reshape.133), calls=%async_computation.2 | async-start | bytes 786432 | tf_op jit(solution)/shard_map/all_to_all | solution.py:150
Sparse Core Ops, SparseCore 0:
  107.2 52.1 all-gather.3
  167.4 58.8 all-gather.5
  228.4 40.6 all-gather.7
